TPU v7x, 32 devices: a whole 2x2x4 slice. The times are simulated.
32 devices in a mesh: fs: 4 (over y, x), tp: 8 (over z, core).
Axes of the slice: x: 2, y: 2, z: 4, core: 2. Of those that a mesh axis runs over, the one named last changes fastest.
Arguments:
- inputs: bfloat16 [8, 320, 2048], P('tp'), may hold values from -6 to 6
- cotangent: bfloat16 [8, 320, 2048], P('tp'), may hold values from -8 to 8
- gate_weight: bfloat16 [2048, 5632], P('tp', 'fs'), may hold values from -0.125 to 0.125
- up_weight: bfloat16 [2048, 5632], P('tp', 'fs'), may hold values from -0.125 to 0.125
- down_weight: bfloat16 [5632, 2048], P('fs', 'tp'), may hold values from -0.078125 to 0.078125
Outputs:
- input_grad: bfloat16 [8, 320, 2048], P('tp')
- down_grad: float32 [5632, 2048], P('fs', 'tp')
All inputs are finite; a program needn't handle non-finite values.
Results may differ from a plain program's by a relative error of at most 0.023.
Values may be sent and summed in bfloat16 or wider, within the bound.
A program may use at most 64 MiB of HBM per device.

v0:
```python
import jax
import jax.numpy as jnp
from jax import lax
from jax.sharding import PartitionSpec as P


def contract_hidden(left, right):
    return lax.dot_general(
        left, right, (((1,), (1,)), ((), ())), preferred_element_type=jnp.float32
    )


def contract_tokens(left, right):
    return lax.dot_general(
        left, right, (((0,), (0,)), ((), ())), preferred_element_type=jnp.float32
    )


def per_device(inputs, cotangent, gate_weight, up_weight, down_weight):
    rows_in = inputs[0]
    rows_grad = cotangent[0]
    token_count = rows_in.shape[0]
    model_width = rows_in.shape[1]
    gate_full, up_full, down_tall = (
        lax.all_gather(gate_weight, "tp", axis=0, tiled=True),
        lax.all_gather(up_weight, "tp", axis=0, tiled=True),
        lax.all_gather(down_weight.T, "tp", axis=0, tiled=True),
    )
    gate_pre = jnp.dot(rows_in, gate_full, preferred_element_type=jnp.float32)
    up_pre = jnp.dot(rows_in, up_full, preferred_element_type=jnp.float32)
    sig = jax.nn.sigmoid(gate_pre)
    hidden = (gate_pre * sig * up_pre).astype(jnp.bfloat16)
    hidden_grad = jnp.dot(rows_grad, down_tall, preferred_element_type=jnp.float32)
    gate_grad = (hidden_grad * up_pre * sig * (1.0 + gate_pre * (1.0 - sig))).astype(jnp.bfloat16)
    up_grad = (hidden_grad * gate_pre * sig).astype(jnp.bfloat16)
    partial_down = contract_tokens(hidden, rows_grad)
    down_grad = lax.psum_scatter(
        partial_down.astype(jnp.bfloat16), "tp", scatter_dimension=1, tiled=True
    ).astype(jnp.float32)
    own_sum = lax.psum_scatter(
        (contract_hidden(gate_grad, gate_full) + contract_hidden(up_grad, up_full)).astype(
            jnp.bfloat16
        ),
        "fs",
        scatter_dimension=0,
        tiled=True,
    )
    whole_grad = lax.all_gather(own_sum, "fs", axis=0, tiled=True)
    input_grad = whole_grad.reshape(1, token_count, model_width)
    return (input_grad, down_grad)


def solution(mesh):
    return jax.shard_map(
        per_device,
        mesh=mesh,
        in_specs=(
            P("tp", None, None),
            P("tp", None, None),
            P("tp", "fs"),
            P("tp", "fs"),
            P("fs", "tp"),
        ),
        out_specs=(P("tp", None, None), P("fs", "tp")),
        check_vma=False,
    )
```

profile of v0, /device:TPU:8, one launch (start us, length us, event | category | flops | bytes accessed | tf_op | source)
XLA Modules:
  0.0 338.2 jit_solution(16475560544088254756)
XLA Ops:
  7.2 0.0 copy-start
  7.2 0.0 copy-start.3
  7.2 0.0 all-gather.9.cloned.1.call-start
  7.2 0.7 all-gather.9.cloned.1.call-update
  7.9 0.0 all-gather.7.cloned.1.call-start
  8.0 0.7 all-gather.7.cloned.1.call-update
  8.7 0.0 all-gather.5.cloned.1.call-start
  8.7 0.7 all-gather.5.cloned.1.call-update
  9.4 0.0 reduce-scatter.3.cloned.1.call-start
  9.5 59.9 %all-gather.9.cloned.1.call-done = bf16[2048,1408]{1,0:T(8,128)(2,1)} async-done(((bf16[256,1408]{1,0:T(8,128)(2,1)}), bf16[2048,1408]{1,0:T(8,128)(2,1)}) %all-gather.9.cloned.1.call-update) | async-done | bytes 5767184 | tf_op jit(solution)/shard_map/all_gather | solution.py:25
  69.3 0.0 copy-done.3
  69.3 6.1 %fusion.1 = f32[320,1408]{1,0:T(8,128)} fusion(bf16[2048,1408]{1,0:T(8,128)(2,1)} %all-gather.9.cloned.1.call-done, bf16[1,320,2048]{2,1,0:T(8,128)(2,1)S(1)} %copy-done.3), kind=kOutput, calls=%fused_computation.7 | convolution fusion | flops 1845493760 | bytes 8880128 | tf_op jit(solution)/shard_map/dot_general | solution.py:29
  75.4 54.6 %all-gather.7.cloned.1.call-done = bf16[2048,1408]{1,0:T(8,128)(2,1)} async-done(((bf16[256,1408]{1,0:T(8,128)(2,1)}), bf16[2048,1408]{1,0:T(8,128)(2,1)}) %all-gather.7.cloned.1.call-update) | async-done | bytes 5767184 | tf_op jit(solution)/shard_map/all_gather | solution.py:26
  130.0 6.1 %fusion.3 = f32[320,1408]{1,0:T(8,128)} fusion(bf16[2048,1408]{1,0:T(8,128)(2,1)} %all-gather.7.cloned.1.call-done, bf16[1,320,2048]{2,1,0:T(8,128)(2,1)S(1)} %copy-done.3), kind=kOutput, calls=%fused_computation.9 | convolution fusion | flops 1845493760 | bytes 8880128 | tf_op jit(solution)/shard_map/dot_general | solution.py:30
  136.1 54.0 %all-gather.5.cloned.1.call-done = bf16[2048,1408]{0,1:T(8,128)(2,1)} async-done(((bf16[256,1408]{0,1:T(8,128)(2,1)}), bf16[2048,1408]{0,1:T(8,128)(2,1)}) %all-gather.5.cloned.1.call-update) | async-done | bytes 5767184 | tf_op jit(solution)/shard_map/all_gather | solution.py:27
  190.1 0.0 copy-done
  190.1 5.0 %fusion.6 = f32[320,1408]{1,0:T(8,128)S(1)} fusion(bf16[2048,1408]{0,1:T(8,128)(2,1)} %all-gather.5.cloned.1.call-done, bf16[1,320,2048]{2,1,0:T(8,128)(2,1)S(1)} %copy-done), kind=kOutput, calls=%fused_computation.12 | convolution fusion | flops 1845493760 | bytes 8880128 | tf_op jit(solution)/shard_map/dot_general | solution.py:33
  195.1 0.0 slice-start.1
  195.1 4.1 %fusion.8 = f32[320,2048]{1,0:T(8,128)S(1)} fusion(bf16[2048,1408]{1,0:T(8,128)(2,1)S(1)} %copy-done.2, f32[320,1408]{1,0:T(8,128)S(1)} %copy-done.4, f32[320,1408]{1,0:T(8,128)S(1)} %fusion.6, f32[320,1408]{1,0:T(8,128)} %fusion.3), kind=kOutput, calls=%fused_computation.14 | convolution fusion | flops 1849999360 | bytes 13795328 | tf_op jit(solution)/shard_map/dot_general | solution.py:8
  199.3 3.4 fusion
  202.7 0.0 reduce-scatter.3.cloned.1.call-update
  202.7 0.0 all-gather.11.cloned.1.call-start
  202.7 30.7 %reduce-scatter.3.cloned.1.call-done = bf16[80,2048]{1,0:T(8,128)(2,1)} async-done(((bf16[320,2048]{1,0:T(8,128)(2,1)}), bf16[80,2048]{1,0:T(8,128)(2,1)}) %reduce-scatter.3.cloned.1.call-update) | async-done | bytes 327696 | tf_op jit(solution)/shard_map/reduce_scatter | solution.py:40
  233.5 0.0 all-gather.11.cloned.1.call-update
  233.5 0.0 reduce-scatter.5.cloned.1.call-start
  233.5 6.7 %convolution_convert_fusion = bf16[1408,2048]{1,0:T(8,128)(2,1)} fusion(bf16[1,320,2048]{2,1,0:T(8,128)(2,1)S(1)} %copy-done, f32[320,1408]{1,0:T(8,128)} %fusion.3, f32[320,1408]{1,0:T(8,128)S(1)} %copy-done.4), kind=kOutput, calls=%fused_computation | convolution fusion | flops 1851080704 | bytes 10682368 | tf_op jit(solution)/shard_map/dot_general | solution.py:14
  240.2 0.0 reduce-scatter.5.cloned.1.call-update
  240.3 23.6 %all-gather.11.cloned.1.call-done = bf16[320,2048]{1,0:T(8,128)(2,1)} async-done(((bf16[80,2048]{1,0:T(8,128)(2,1)}), bf16[320,2048]{1,0:T(8,128)(2,1)}) %all-gather.11.cloned.1.call-update) | async-done | bytes 1310736 | tf_op jit(solution)/shard_map/all_gather | solution.py:48
  263.9 64.2 %reduce-scatter.5.cloned.1.call-done = bf16[1408,256]{1,0:T(8,128)(2,1)} async-done(((bf16[1408,2048]{1,0:T(8,128)(2,1)}), bf16[1408,256]{1,0:T(8,128)(2,1)}) %reduce-scatter.5.cloned.1.call-update) | async-done | bytes 720912 | tf_op jit(solution)/shard_map/reduce_scatter | solution.py:37
  328.0 2.3 convert_element_type.23
  330.3 0.0 copy-done.1
  330.3 1.1 copy.8
  (9 shorter events, 0.0 us)
Async XLA Ops:
  7.2 182.9 %copy-start = (bf16[1,320,2048]{2,1,0:T(8,128)(2,1)S(1)}, bf16[1,320,2048]{2,1,0:T(8,128)(2,1)}, u32[]{:S(2)}) copy-start(bf16[1,320,2048]{2,1,0:T(8,128)(2,1)} %param.6) | copy-start | bytes 3932164
  7.2 62.1 %copy-start.3 = (bf16[1,320,2048]{2,1,0:T(8,128)(2,1)S(1)}, bf16[1,320,2048]{2,1,0:T(8,128)(2,1)}, u32[]{:S(2)}) copy-start(bf16[1,320,2048]{2,1,0:T(8,128)(2,1)} %param.5) | copy-start | bytes 3932164
  7.2 62.1 %all-gather.9.cloned.1.call-start = ((), (), s32[]{:S(2)}) async-start(), calls=%async_computation.4 | async-start | bytes 6488064 | tf_op jit(solution)/shard_map/all_gather | solution.py:25
  7.9 122.1 %all-gather.7.cloned.1.call-start = ((), (), s32[]{:S(2)}) async-start(), calls=%async_computation.3 | async-start | bytes 6488064 | tf_op jit(solution)/shard_map/all_gather | solution.py:26
  8.7 181.4 %all-gather.5.cloned.1.call-start = ((), (), s32[]{:S(2)}) async-start(), calls=%async_computation.2 | async-start | bytes 6488064 | tf_op jit(solution)/shard_map/all_gather | solution.py:27
  9.4 224.1 %reduce-scatter.3.cloned.1.call-start = ((), (), s32[]{:S(2)}) async-start(), calls=%async_computation.5 | async-start | bytes 1638400 | tf_op jit(solution)/shard_map/reduce_scatter | solution.py:40
  136.1 59.0 %copy-start.4 = (f32[320,1408]{1,0:T(8,128)S(1)}, f32[320,1408]{1,0:T(8,128)}, u32[]{:S(2)}) copy-start(f32[320,1408]{1,0:T(8,128)} %fusion.1) | copy-start | bytes 5406724
  190.1 5.0 %copy-start.2 = (bf16[2048,1408]{1,0:T(8,128)(2,1)S(1)}, bf16[2048,1408]{1,0:T(8,128)(2,1)}, u32[]{:S(2)}) copy-start(bf16[2048,1408]{1,0:T(8,128)(2,1)} %all-gather.9.cloned.1.call-done) | copy-start | bytes 17301508
  190.1 9.2 %slice-start = ((s8[5767168]{0:T(1024)(128)(4,1)}), s8[4194304]{0:T(1024)(128)(4,1)S(1)}, s32[]{:S(2)}) async-start(s8[5767168]{0:T(1024)(128)(4,1)} %bitcast.19), calls=%async_computation.8 | async-start | bytes 8388608
  195.1 4.2 %slice-start.1 = ((s8[5767168]{0:T(1024)(128)(4,1)}), s8[1572864]{0:T(1024)(128)(4,1)S(1)}, s32[]{:S(2)}) async-start(s8[5767168]{0:T(1024)(128)(4,1)} %bitcast.19), calls=%async_computation.9 | async-start | bytes 3145728
  202.7 61.2 %all-gather.11.cloned.1.call-start = ((), (), s32[]{:S(2)}) async-start(), calls=%async_computation.6 | async-start | bytes 1638400 | tf_op jit(solution)/shard_map/all_gather | solution.py:48
  233.5 94.5 %reduce-scatter.5.cloned.1.call-start = ((), (), s32[]{:S(2)}) async-start(), calls=%async_computation.7 | async-start | bytes 6488064 | tf_op jit(solution)/shard_map/reduce_scatter | solution.py:37
  263.9 66.5 %copy-start.1 = (bf16[320,2048]{1,0:T(8,128)(2,1)S(1)}, bf16[320,2048]{1,0:T(8,128)(2,1)}, u32[]{:S(2)}) copy-start(bf16[320,2048]{1,0:T(8,128)(2,1)} %all-gather.11.cloned.1.call-done) | copy-start | bytes 3932164
Sparse Core Ops, SparseCore 0:
  9.6 59.6 all-gather.8
  71.0 59.0 all-gather.6
  131.6 58.3 all-gather.4
  202.8 30.6 reduce-scatter.2
  235.2 28.6 all-gather.10
  266.0 61.9 reduce-scatter.4
where the time goes:
time: 343 us; the launch traced here: 338 us
  waiting for transfers between devices  289 us (84%)
  matrix products  31.4 us (9%)
  between operations  14.2 us (4%)
    reduce_scatter x1, waiting for transfers between devices, per_device(): lax.psum_scatter(partial_down.astype(jnp.bfloat16), 'tp', scatter_dimensi...  64.2 us
    all_gather x1, waiting for transfers between devices, per_device(): lax.all_gather(gate_weight, 'tp', axis=0, tiled=True)  59.9 us
    all_gather x1, waiting for transfers between devices, per_device(): lax.all_gather(up_weight, 'tp', axis=0, tiled=True)  54.6 us
    all_gather x1, waiting for transfers between devices, per_device(): lax.all_gather(down_weight.T, 'tp', axis=0, tiled=True)  54 us
    reduce_scatter x1, waiting for transfers between devices, per_device(): lax.psum_scatter((contract_hidden(gate_grad, gate_full) + contract_hidden...  30.7 us
    all_gather x1, waiting for transfers between devices, per_device(): whole_grad = lax.all_gather(own_sum, 'fs', axis=0, tiled=True)  23.6 us
    dot_general x2, matrix products, contract_hidden(): lax.dot_general(left, right, (((1,), (1,)), ((), ())), preferred_element_...  7.51 us
  transfers between devices with their start and end apart: 6, of which 6 were waited for; matrix products, arithmetic and copies ran while one was open for 6% of the time, Pallas kernels for 0%

commit v1 on v0

v1 whole, which is shorter than its diff:
```python
import functools

import jax
import jax.numpy as jnp
from jax import lax
from jax.experimental import pallas as pl
from jax.experimental.pallas import tpu as pltpu
from jax.sharding import PartitionSpec as P

MESH = pl.DeviceIdType.MESH
BF16 = jnp.bfloat16
F32 = jnp.float32


def contract_hidden(left, right):
    return lax.dot_general(left, right, (((1,), (1,)), ((), ())), preferred_element_type=F32)


def contract_tokens(left, right):
    return lax.dot_general(left, right, (((0,), (0,)), ((), ())), preferred_element_type=F32)


def gathered(inputs, cotangent, gate_weight, up_weight, down_weight):
    rows_in = inputs[0]
    rows_grad = cotangent[0]
    token_count, model_width = rows_in.shape
    gate_full = lax.all_gather(gate_weight, "tp", axis=0, tiled=True)
    up_full = lax.all_gather(up_weight, "tp", axis=0, tiled=True)
    down_tall = lax.all_gather(down_weight.T, "tp", axis=0, tiled=True)
    gate_pre = jnp.dot(rows_in, gate_full, preferred_element_type=F32)
    up_pre = jnp.dot(rows_in, up_full, preferred_element_type=F32)
    sig = jax.nn.sigmoid(gate_pre)
    hidden = (gate_pre * sig * up_pre).astype(BF16)
    hidden_grad = jnp.dot(rows_grad, down_tall, preferred_element_type=F32)
    gate_grad = (hidden_grad * up_pre * sig * (1.0 + gate_pre * (1.0 - sig))).astype(BF16)
    up_grad = (hidden_grad * gate_pre * sig).astype(BF16)
    partial_down = contract_tokens(hidden, rows_grad)
    down_grad = lax.psum_scatter(
        partial_down.astype(BF16), "tp", scatter_dimension=1, tiled=True
    ).astype(F32)
    own_sum = lax.psum_scatter(
        (contract_hidden(gate_grad, gate_full) + contract_hidden(up_grad, up_full)).astype(BF16),
        "fs",
        scatter_dimension=0,
        tiled=True,
    )
    whole_grad = lax.all_gather(own_sum, "fs", axis=0, tiled=True)
    return (whole_grad.reshape(1, token_count, model_width), down_grad)


def kernel(
    n_tp, x_ref, ct_ref, wg_ref, wu_ref, wd_ref, grad_ref, down_ref,
    tok, part, core_in, half_in, quarter_in, chain_in, wts, acc, down_out, down_in,
    loc_sem, tok_rs, z_ss, xy_ss, dg_ss, d2d_ss, d2d_rs, w_ss, w_rs, core_ss, core_rs,
    half_ss, half_rs, q_ss, q_rs, ch_ss, ch_rs, ag_ss, ag_rs, dn_ss, dn_rs,
):
    f, t = lax.axis_index("fs"), lax.axis_index("tp")
    n_z = n_tp // 2
    z, c = t // 2, t % 2
    fy, fx = f // 2, f % 2
    f_x = fy * 2 + (1 - fx)
    f_y = (1 - fy) * 2 + fx
    f_d = (1 - fy) * 2 + (1 - fx)
    dev_x, dev_y, dev_d = {"fs": f_x}, {"fs": f_y}, {"fs": f_d}
    partner = {"tp": z * 2 + (1 - c)}
    n_tok, width = tok.shape[2], tok.shape[3]
    qr = n_tok // 4
    hid = wts.shape[1]
    cols = width // n_tp

    def plane(delta):
        return {"tp": (z + delta) * 2 + c}

    def rc(src, dst, ss, rs, dev):
        return pltpu.make_async_remote_copy(
            src_ref=src, dst_ref=dst, send_sem=ss, recv_sem=rs, device_id=dev, device_id_type=MESH
        )

    def qs(q):
        return pl.ds(pl.multiple_of(q * qr, qr), qr)

    def tokq(arr, span, q):
        return tok.at[arr, span, qs(q)]

    own = [
        pltpu.make_async_copy(x_ref.at[0], tok.at[0, t], loc_sem.at[0]),
        pltpu.make_async_copy(ct_ref.at[0], tok.at[1, t], loc_sem.at[1]),
    ]
    own_cols = pl.ds(pl.multiple_of(t * cols, cols), cols)
    for i, w in enumerate((wg_ref, wu_ref, wd_ref)):
        own.append(
            pltpu.make_async_copy(
                w.at[pl.ds(pl.multiple_of(t * hid, hid), hid)], wts.at[i, :, own_cols], loc_sem.at[2 + i]
            )
        )
    for copy in own:
        copy.start()

    barrier = pltpu.get_barrier_semaphore()
    for dev in (dev_x, dev_y, dev_d):
        pl.semaphore_signal(barrier, inc=1, device_id=dev, device_id_type=MESH)
    for k in range(1, n_tp):
        pl.semaphore_signal(barrier, inc=1, device_id={"tp": (t + k) % n_tp}, device_id_type=MESH)
    pl.semaphore_wait(barrier, 3 + n_tp - 1)
    for copy in own:
        copy.wait()

    def z_copy(arr, p, d):
        src = tokq(arr, p * 2 + c, f)
        return rc(src, src, z_ss.at[arr, p, d], tok_rs.at[arr, p, f], plane(1 if d else -1))

    def xy_copy(arr, p, d):
        src = tokq(arr, p * 2 + c, f)
        return rc(src, src, xy_ss.at[arr, p, d], tok_rs.at[arr, p, f], dev_y if d else dev_x)

    def relay_copy(arr, p):
        q = f_y if arr else f_x
        src = tokq(arr, p * 2 + c, q)
        return rc(src, src, dg_ss.at[arr, p], tok_rs.at[arr, p, q], dev_x if arr else dev_y)

    def tok_wait(arr, p, q):
        dst = tokq(arr, p * 2 + c, q)
        rc(dst, dst, z_ss.at[arr, p, 0], tok_rs.at[arr, p, q], dev_x).wait_recv()

    def d2d_copy(arr, p, core):
        src = tok.at[arr, p * 2 + core]
        return rc(src, src, d2d_ss.at[arr, p], d2d_rs.at[arr, p], partner)

    def w_copy(i, k):
        to = (t + k) % n_tp
        return rc(
            (wg_ref, wu_ref, wd_ref)[i].at[pl.ds(pl.multiple_of(to * hid, hid), hid)],
            wts.at[i, :, own_cols], w_ss.at[i, k], w_rs.at[i, k], {"tp": to},
        )

    for arr in range(2):
        for d, ok in ((1, z < n_z - 1), (0, z > 0)):
            @pl.when(ok)
            def _(arr=arr, d=d):
                z_copy(arr, z, d).start()
        d2d_copy(arr, z, c).start()

    w_order = list(range(1, n_tp))
    for step in range(1, n_z):
        for i in range(3):
            for k in w_order[(step - 1) * len(w_order) // (n_z - 1):step * len(w_order) // (n_z - 1)]:
                w_copy(i, k).start()
        for d in (1, 0):
            p = z - step if d else z + step

            @pl.when((p >= 0) & (p < n_z))
            def _(p=p, d=d):
                for arr in range(2):
                    tok_wait(arr, p, f)

                    @pl.when(z < n_z - 1 if d else z > 0)
                    def _():
                        z_copy(arr, p, d).start()

                    xy_copy(arr, p, 0).start()
                    xy_copy(arr, p, 1).start()

    def order(j):
        return jnp.where(z < n_z // 2, z + j, z - j + n_z) % n_z

    @pl.loop(1, n_z)
    def _(j):
        p = order(j)
        tok_wait(0, p, f_x)
        relay_copy(0, p).start()
        tok_wait(1, p, f_y)
        relay_copy(1, p).start()

    @pl.loop(1, n_z)
    def _(j):
        p = order(j)
        tok_wait(0, p, f_y)
        tok_wait(0, p, f_d)
        d2d_copy(0, p, c).start()
        tok_wait(1, p, f_x)
        tok_wait(1, p, f_d)
        d2d_copy(1, p, c).start()

    for i in range(3):
        for k in range(1, n_tp):
            frm = (t - k + n_tp) % n_tp
            dst = wts.at[i, :, pl.ds(pl.multiple_of(frm * cols, cols), cols)]
            rc(dst, dst, w_ss.at[i, k], w_rs.at[i, k], partner).wait_recv()

    acc[...] = jnp.zeros_like(acc)

    def core_copy(p):
        return rc(part.at[p * 2 + 1 - c], core_in.at[p], core_ss.at[p], core_rs.at[p], partner)

    def half_copy(p, first_x, i):
        q = jnp.where(first_x, i * 2 + (1 - fx), (1 - fy) * 2 + i)
        dev = {"fs": jnp.where(first_x, f_x, f_y)}
        return rc(part.at[p * 2 + c, qs(q)], half_in.at[p, i], half_ss.at[p, i], half_rs.at[p, i], dev)

    @pl.loop(0, n_z)
    def _(j):
        p = order(j)
        for arr in range(2):
            dst = tok.at[arr, p * 2 + 1 - c]
            rc(dst, dst, d2d_ss.at[arr, p], d2d_rs.at[arr, p], partner).wait_recv()

        @pl.loop(0, 2)
        def _(u):
            s = p * 2 + jnp.where(u == 0, 1 - c, c)
            rows, ct = tok[0, s], tok[1, s]
            gate_pre = contract_hidden(rows, wts[0])
            up_pre = contract_hidden(rows, wts[1])
            hidden_grad = contract_hidden(ct, wts[2])
            sig = jax.nn.sigmoid(gate_pre)
            silu = gate_pre * sig
            hidden = (silu * up_pre).astype(BF16)
            gate_grad = (hidden_grad * up_pre * sig * (1.0 + gate_pre * (1.0 - sig))).astype(BF16)
            up_grad = (hidden_grad * silu).astype(BF16)
            acc[...] += contract_tokens(hidden, ct)
            part[s] = (
                jnp.dot(gate_grad, wts[0], preferred_element_type=F32)
                + jnp.dot(up_grad, wts[1], preferred_element_type=F32)
            ).astype(BF16)

            @pl.when(u == 0)
            def _():
                core_copy(p).start()

        core_copy(p).wait_recv()
        s = p * 2 + c
        part[s] = (part[s].astype(F32) + core_in[p].astype(F32)).astype(BF16)
        first_x = p % 2 == 0
        half_copy(p, first_x, 0).start()
        half_copy(p, first_x, 1).start()

    down_out[...] = acc[...].astype(BF16)

    def dn_copy(k):
        to = (t + k) % n_tp
        return rc(
            down_out.at[:, pl.ds(pl.multiple_of(to * cols, cols), cols)],
            down_in.at[pl.ds(pl.multiple_of(t * hid, hid), hid)],
            dn_ss.at[k], dn_rs.at[k], {"tp": to},
        )

    for k in range(1, n_tp):
        dn_copy(k).start()

    def quarter_copy(p, first_x):
        q = jnp.where(first_x, f_y, f_x)
        return rc(
            part.at[p * 2 + c, qs(q)], quarter_in.at[p], q_ss.at[p], q_rs.at[p],
            {"fs": jnp.where(first_x, f_y, f_x)},
        )

    @pl.loop(0, n_z)
    def _(j):
        p = order(j)
        first_x = p % 2 == 0
        s = p * 2 + c
        other = jnp.where(first_x, 1 - fy, 1 - fx)
        mine = jnp.where(first_x, fy, fx)
        for i in range(2):
            half_copy(p, first_x, i).wait_recv()
        q_other = jnp.where(first_x, f_y, f_x)
        part[s, qs(q_other)] = (
            part[s, qs(q_other)].astype(F32) + half_in[p, other].astype(F32)
        ).astype(BF16)
        quarter_copy(p, first_x).start()
        part[s, qs(f)] = (part[s, qs(f)].astype(F32) + half_in[p, mine].astype(F32)).astype(BF16)

    @pl.loop(0, n_z)
    def _(j):
        p = order(j)
        quarter_copy(p, p % 2 == 0).wait_recv()
        s = p * 2 + c
        part[s, qs(f)] = (part[s, qs(f)].astype(F32) + quarter_in[p].astype(F32)).astype(BF16)

    def chain_copy(p, d):
        return rc(
            part.at[p * 2 + c, qs(f)], chain_in.at[p, d], ch_ss.at[p], ch_rs.at[p, d],
            plane(1 if d else -1),
        )

    def chain_add(p, d):
        chain_copy(p, d).wait_recv()
        s = p * 2 + c
        part[s, qs(f)] = (part[s, qs(f)].astype(F32) + chain_in[p, d].astype(F32)).astype(BF16)

    for step in range(n_z - 1, 0, -1):
        for d in (1, 0):
            p = z + step if d else z - step

            @pl.when((p >= 0) & (p < n_z))
            def _(p=p, d=d):
                @pl.when(z > 0 if d else z < n_z - 1)
                def _():
                    chain_add(p, d)

                chain_copy(p, d).start()

    @pl.when(z > 0)
    def _():
        chain_add(z, 1)

    @pl.when(z < n_z - 1)
    def _():
        chain_add(z, 0)

    grad_ref[0, qs(f)] = part[t, qs(f)]

    def ag_copy(i, q):
        return rc(
            part.at[t, qs(f)], grad_ref.at[0, qs(q)], ag_ss.at[i], ag_rs.at[i], (dev_x, dev_y, dev_d)[i]
        )

    for i in (2, 0, 1):
        ag_copy(i, f).start()

    down_ref[pl.ds(pl.multiple_of(t * hid, hid), hid)] = acc[:, own_cols]
    for k in range(1, n_tp):
        frm = (t - k + n_tp) % n_tp
        rows = pl.ds(pl.multiple_of(frm * hid, hid), hid)
        rc(down_in.at[rows], down_in.at[rows], dn_ss.at[k], dn_rs.at[k], partner).wait_recv()
        down_ref[rows] = down_in[rows].astype(F32)

    for i, q in enumerate((f_x, f_y, f_d)):
        ag_copy(i, q).wait_recv()

    for arr in range(2):
        for p in range(n_z):
            @pl.when((z < n_z - 1) & (p <= z))
            def _(arr=arr, p=p):
                z_copy(arr, p, 1).wait_send()

            @pl.when((z > 0) & (p >= z))
            def _(arr=arr, p=p):
                z_copy(arr, p, 0).wait_send()

            d2d_copy(arr, p, c).wait_send()

            @pl.when(p != z)
            def _(arr=arr, p=p):
                xy_copy(arr, p, 0).wait_send()
                xy_copy(arr, p, 1).wait_send()
                relay_copy(arr, p).wait_send()

    for k in range(1, n_tp):
        for i in range(3):
            w_copy(i, k).wait_send()
        dn_copy(k).wait_send()
    for p in range(n_z):
        core_copy(p).wait_send()
        half_copy(p, p % 2 == 0, 0).wait_send()
        half_copy(p, p % 2 == 0, 1).wait_send()
        quarter_copy(p, p % 2 == 0).wait_send()

        @pl.when(p != z)
        def _(p=p):
            chain_copy(p, 0).wait_send()

    for i in range(3):
        ag_copy(i, f).wait_send()


def spread(n_tp, inputs, cotangent, gate_weight, up_weight, down_weight):
    _, n_tok, width = inputs.shape
    hid_all = gate_weight.shape[1]
    hid, cols, n_z, qr = hid_all // n_tp, width // n_tp, n_tp // 2, n_tok // 4
    dma = pltpu.SemaphoreType.DMA
    vmem = pl.BlockSpec(memory_space=pltpu.VMEM)
    anyspace = pl.BlockSpec(memory_space=pl.ANY)
    return pl.pallas_call(
        functools.partial(kernel, n_tp),
        name="spread_hidden",
        out_shape=(
            jax.ShapeDtypeStruct((1, n_tok, width), BF16),
            jax.ShapeDtypeStruct((hid_all, cols), F32),
        ),
        in_specs=[anyspace, anyspace, vmem, vmem, vmem],
        out_specs=(vmem, vmem),
        scratch_shapes=[
            pltpu.VMEM((2, n_tp, n_tok, width), BF16),
            pltpu.VMEM((n_tp, n_tok, width), BF16),
            pltpu.VMEM((n_z, n_tok, width), BF16),
            pltpu.VMEM((n_z, 2, qr, width), BF16),
            pltpu.VMEM((n_z, qr, width), BF16),
            pltpu.VMEM((n_z, 2, qr, width), BF16),
            pltpu.VMEM((3, hid, width), BF16),
            pltpu.VMEM((hid, width), F32),
            pltpu.VMEM((hid, width), BF16),
            pltpu.VMEM((hid_all, cols), BF16),
            dma((5,)), dma((2, n_z, 4)), dma((2, n_z, 2)), dma((2, n_z, 2)), dma((2, n_z)),
            dma((2, n_z)), dma((2, n_z)), dma((3, n_tp)), dma((3, n_tp)), dma((n_z,)), dma((n_z,)),
            dma((n_z, 2)), dma((n_z, 2)), dma((n_z,)), dma((n_z,)), dma((n_z,)), dma((n_z, 2)),
            dma((3,)), dma((3,)), dma((n_tp,)), dma((n_tp,)),
        ],
        compiler_params=pltpu.CompilerParams(
            collective_id=0, has_side_effects=True, vmem_limit_bytes=66_000_000
        ),
    )(inputs, cotangent, gate_weight.T, up_weight.T, down_weight)


def solution(mesh):
    n_fs, n_tp = mesh.shape["fs"], mesh.shape["tp"]

    def per_device(inputs, cotangent, gate_weight, up_weight, down_weight):
        _, n_tok, width = inputs.shape
        hid_all = gate_weight.shape[1]
        n_z = n_tp // 2
        fits = (
            n_fs == 4
            and n_tp % 2 == 0
            and hid_all % (n_tp * 16) == 0
            and width % (n_tp * 128) == 0
            and n_tok % 64 == 0
            and 2 * n_tok * width * (3 * n_tp + 3 * n_z + 4) + 16 * hid_all * width < 62_000_000 * 2
        )
        if not fits:
            return gathered(inputs, cotangent, gate_weight, up_weight, down_weight)
        return spread(n_tp, inputs, cotangent, gate_weight, up_weight, down_weight)

    return jax.shard_map(
        per_device,
        mesh=mesh,
        in_specs=(
            P("tp", None, None),
            P("tp", None, None),
            P("tp", "fs"),
            P("tp", "fs"),
            P("fs", "tp"),
        ),
        out_specs=(P("tp", None, None), P("fs", "tp")),
        check_vma=False,
    )
```

time: 343 us -> 222 us (0.65)
  waiting for transfers between devices: 289 us -> 0 us
  Pallas kernels: 0 us -> 212 us
  matrix products: 31.4 us -> 0 us
  between operations: 14.2 us -> 0.66 us
  local copies, waits for them, and re-layouts: 1.09 us -> 7.19 us
    pallas_call x0 -> x1, Pallas kernels: none -> 212 us  [spread(): pl.pallas_call(functools.partial(kernel, n_tp), name='spread_hidden', out...]
    all_gather x4 -> x0, waiting for transfers between devices: 192 us -> none  [the longest x1 59.9 us: per_device(): lax.all_gather(gate_weight, 'tp', axis=0, tiled=True)]
    reduce_scatter x2 -> x0, waiting for transfers between devices: 94.9 us -> none  [the longest x1 64.2 us: per_device(): lax.psum_scatter(partial_down.astype(jnp.bfloat16), 'tp', scatter_dimensi...]
    dot_general x6 -> x0, matrix products: 31.4 us -> none  [the longest x2 7.51 us: contract_hidden(): lax.dot_general(left, right, (((1,), (1,)), ((), ())), preferred_element_...]
    unnamed x15 -> x8, local copies, waits for them, and re-layouts: 1.09 us -> 7.19 us
  transfers between devices with their start and end apart: 6 -> 0, of which waited for: 6 -> 0; matrix products, arithmetic and copies ran while one was open for 6% -> 0% of each run, Pallas kernels for 0% -> 0%
where the time goes in v1:
time: 222 us; the launch traced here: 220 us
  Pallas kernels  212 us (95%)
  local copies, waits for them, and re-layouts  7.19 us (3%)
    pallas_call x1, Pallas kernels, spread(): pl.pallas_call(functools.partial(kernel, n_tp), name='spread_hidden', out...  212 us
    unnamed x8, local copies, waits for them, and re-layouts  7.19 us

profile of v1, /device:TPU:8, one launch (start us, length us, event | category | flops | bytes accessed | tf_op | source)
XLA Modules:
  0.0 220.0 jit_solution(16952869963233997778)
XLA Ops:
  0.6 0.0 copy-start.1
  0.6 2.3 %copy.7 = bf16[256,1408]{0,1:T(8,128)(2,1)} copy(bf16[256,1408]{1,0:T(8,128)(2,1)} %param.7) | data formatting | bytes 1441792 | tf_op args[2]
  3.0 0.0 copy-done.1
  3.0 1.1 copy.8
  4.1 212.2 %spread_hidden.1 = (bf16[1,320,2048]{2,1,0:T(8,128)(2,1)}, f32[1408,256]{1,0:T(8,128)}) custom-call(bf16[1,320,2048]{2,1,0:T(8,128)(2,1)} %x_ref.1, bf16[1,320,2048]{2,1,0:T(8,128)(2,1)} %ct_ref.1, bf16[1408,256]{1,0:T(8,128)(2,1)} %bitcast.2, bf16[1408,256]{1,0:T(8,128)(2,1)} %bitcast.3, bf16[1408,256]{1,0:T(8,128)(2,1)} %wd_ref.1), custom_call_target="tpu_custom_call" | custom-call | tf_op jit(solution)/shard_map/spread_hidden/pallas_call | solution.py:373
  216.3 0.0 copy-start
  216.3 2.6 %copy.11 = bf16[1,320,2048]{2,1,0:T(8,128)(2,1)} copy(bf16[1,320,2048]{2,1,0:T(8,128)(2,1)} %get-tuple-element.4) | data formatting | bytes 2621440
  218.9 0.0 copy-done
  218.9 1.1 copy.12
Async XLA Ops:
  0.6 2.3 %copy-start.1 = (bf16[256,1408]{1,0:T(8,128)(2,1)S(1)}, bf16[256,1408]{1,0:T(8,128)(2,1)}, u32[]{:S(2)}) copy-start(bf16[256,1408]{1,0:T(8,128)(2,1)} %param.8) | copy-start | bytes 2162692
  216.3 2.6 %copy-start = (f32[1408,256]{1,0:T(8,128)S(1)}, f32[1408,256]{1,0:T(8,128)}, u32[]{:S(2)}) copy-start(f32[1408,256]{1,0:T(8,128)} %get-tuple-element.5) | copy-start | bytes 4325380

commit v2 on v1

--- a/solution.py
+++ b/solution.py
@@ -51,7 +51,7 @@
 def kernel(
     n_tp, x_ref, ct_ref, wg_ref, wu_ref, wd_ref, grad_ref, down_ref,
     tok, part, core_in, half_in, quarter_in, chain_in, wts, acc, down_out, down_in,
-    loc_sem, tok_rs, z_ss, xy_ss, dg_ss, d2d_ss, d2d_rs, w_ss, w_rs, core_ss, core_rs,
+    gate_t, up_t, loc_sem, tok_rs, z_ss, xy_ss, dg_ss, d2d_ss, d2d_rs, w_ss, w_rs, core_ss, core_rs,
     half_ss, half_rs, q_ss, q_rs, ch_ss, ch_rs, ag_ss, ag_rs, dn_ss, dn_rs,
 ):
     f, t = lax.axis_index("fs"), lax.axis_index("tp")
@@ -87,12 +87,6 @@
         pltpu.make_async_copy(ct_ref.at[0], tok.at[1, t], loc_sem.at[1]),
     ]
     own_cols = pl.ds(pl.multiple_of(t * cols, cols), cols)
-    for i, w in enumerate((wg_ref, wu_ref, wd_ref)):
-        own.append(
-            pltpu.make_async_copy(
-                w.at[pl.ds(pl.multiple_of(t * hid, hid), hid)], wts.at[i, :, own_cols], loc_sem.at[2 + i]
-            )
-        )
     for copy in own:
         copy.start()
 
@@ -126,12 +120,21 @@
         src = tok.at[arr, p * 2 + core]
         return rc(src, src, d2d_ss.at[arr, p], d2d_rs.at[arr, p], partner)
 
-    def w_copy(i, k):
-        to = (t + k) % n_tp
+    def w_copy(i, to):
         return rc(
-            (wg_ref, wu_ref, wd_ref)[i].at[pl.ds(pl.multiple_of(to * hid, hid), hid)],
-            wts.at[i, :, own_cols], w_ss.at[i, k], w_rs.at[i, k], {"tp": to},
-        )
+            (gate_t, up_t, wd_ref)[i].at[pl.ds(pl.multiple_of(to * hid, hid), hid)],
+            wts.at[i, :, own_cols], w_ss.at[i, to], w_rs.at[i, t], {"tp": to},
+        )
+
+    def w_send(d):
+        @pl.loop(2, 2 * n_z)
+        def _(k):
+            p = z + k // 2 if d else z - k // 2
+
+            @pl.when((p >= 0) & (p < n_z))
+            def _():
+                for i in range(3):
+                    w_copy(i, p * 2 + k % 2).start()
 
     for arr in range(2):
         for d, ok in ((1, z < n_z - 1), (0, z > 0)):
@@ -140,13 +143,21 @@
                 z_copy(arr, z, d).start()
         d2d_copy(arr, z, c).start()
 
-    w_order = list(range(1, n_tp))
-    for step in range(1, n_z):
-        for i in range(3):
-            for k in w_order[(step - 1) * len(w_order) // (n_z - 1):step * len(w_order) // (n_z - 1)]:
-                w_copy(i, k).start()
+    gate_t[...] = wg_ref[...].T
+    up_t[...] = wu_ref[...].T
+    own_rows = pl.ds(pl.multiple_of(t * hid, hid), hid)
+    for i, w in enumerate((gate_t, up_t, wd_ref)):
+        wts[i, :, own_cols] = w[own_rows]
+
+    for i in range(3):
+        w_copy(i, z * 2 + 1 - c).start()
+
+    for step in range(n_z):
         for d in (1, 0):
             p = z - step if d else z + step
+
+            if step == 0:
+                continue
 
             @pl.when((p >= 0) & (p < n_z))
             def _(p=p, d=d):
@@ -160,8 +171,16 @@
                     xy_copy(arr, p, 0).start()
                     xy_copy(arr, p, 1).start()
 
+        for d in (1, 0):
+            @pl.when((z if d else n_z - 1 - z) == step)
+            def _(d=d):
+                w_send(d)
+
     def order(j):
         return jnp.where(z < n_z // 2, z + j, z - j + n_z) % n_z
+
+    def sweep(j):
+        return jnp.where(j % 2 == 0, n_z - 1 - j // 2, j // 2)
 
     @pl.loop(1, n_z)
     def _(j):
@@ -185,7 +204,7 @@
         for k in range(1, n_tp):
             frm = (t - k + n_tp) % n_tp
             dst = wts.at[i, :, pl.ds(pl.multiple_of(frm * cols, cols), cols)]
-            rc(dst, dst, w_ss.at[i, k], w_rs.at[i, k], partner).wait_recv()
+            rc(dst, dst, w_ss.at[i, frm], w_rs.at[i, frm], partner).wait_recv()
 
     acc[...] = jnp.zeros_like(acc)
 
@@ -199,7 +218,7 @@
 
     @pl.loop(0, n_z)
     def _(j):
-        p = order(j)
+        p = sweep(j)
         for arr in range(2):
             dst = tok.at[arr, p * 2 + 1 - c]
             rc(dst, dst, d2d_ss.at[arr, p], d2d_rs.at[arr, p], partner).wait_recv()
@@ -229,7 +248,7 @@
         core_copy(p).wait_recv()
         s = p * 2 + c
         part[s] = (part[s].astype(F32) + core_in[p].astype(F32)).astype(BF16)
-        first_x = p % 2 == 0
+        first_x = p >= n_z // 2
         half_copy(p, first_x, 0).start()
         half_copy(p, first_x, 1).start()
 
@@ -253,10 +272,8 @@
             {"fs": jnp.where(first_x, f_y, f_x)},
         )
 
-    @pl.loop(0, n_z)
-    def _(j):
-        p = order(j)
-        first_x = p % 2 == 0
+    def half_add(p):
+        first_x = p >= n_z // 2
         s = p * 2 + c
         other = jnp.where(first_x, 1 - fy, 1 - fx)
         mine = jnp.where(first_x, fy, fx)
@@ -269,43 +286,37 @@
         quarter_copy(p, first_x).start()
         part[s, qs(f)] = (part[s, qs(f)].astype(F32) + half_in[p, mine].astype(F32)).astype(BF16)
 
+    def chain_copy(p):
+        return rc(
+            part.at[p * 2 + c, qs(f)], chain_in.at[z], ch_ss.at[p], ch_rs.at[z], {"tp": p * 2 + c}
+        )
+
+    @pl.loop(0, n_z + 1)
+    def _(j):
+        @pl.when(j < n_z)
+        def _():
+            half_add(sweep(j))
+
+        @pl.when(j > 0)
+        def _():
+            p = sweep(j - 1)
+            quarter_copy(p, p >= n_z // 2).wait_recv()
+            s = p * 2 + c
+            part[s, qs(f)] = (part[s, qs(f)].astype(F32) + quarter_in[p].astype(F32)).astype(BF16)
+
+            @pl.when(p != z)
+            def _():
+                chain_copy(p).start()
+
     @pl.loop(0, n_z)
     def _(j):
-        p = order(j)
-        quarter_copy(p, p % 2 == 0).wait_recv()
-        s = p * 2 + c
-        part[s, qs(f)] = (part[s, qs(f)].astype(F32) + quarter_in[p].astype(F32)).astype(BF16)
-
-    def chain_copy(p, d):
-        return rc(
-            part.at[p * 2 + c, qs(f)], chain_in.at[p, d], ch_ss.at[p], ch_rs.at[p, d],
-            plane(1 if d else -1),
-        )
-
-    def chain_add(p, d):
-        chain_copy(p, d).wait_recv()
-        s = p * 2 + c
-        part[s, qs(f)] = (part[s, qs(f)].astype(F32) + chain_in[p, d].astype(F32)).astype(BF16)
-
-    for step in range(n_z - 1, 0, -1):
-        for d in (1, 0):
-            p = z + step if d else z - step
-
-            @pl.when((p >= 0) & (p < n_z))
-            def _(p=p, d=d):
-                @pl.when(z > 0 if d else z < n_z - 1)
-                def _():
-                    chain_add(p, d)
-
-                chain_copy(p, d).start()
-
-    @pl.when(z > 0)
-    def _():
-        chain_add(z, 1)
-
-    @pl.when(z < n_z - 1)
-    def _():
-        chain_add(z, 0)
+        frm = sweep(j)
+
+        @pl.when(frm != z)
+        def _():
+            dst = chain_in.at[frm]
+            rc(dst, dst, ch_ss.at[frm], ch_rs.at[frm], partner).wait_recv()
+            part[t, qs(f)] = (part[t, qs(f)].astype(F32) + dst[...].astype(F32)).astype(BF16)
 
     grad_ref[0, qs(f)] = part[t, qs(f)]
 
@@ -347,17 +358,17 @@
 
     for k in range(1, n_tp):
         for i in range(3):
-            w_copy(i, k).wait_send()
+            w_copy(i, (t + k) % n_tp).wait_send()
         dn_copy(k).wait_send()
     for p in range(n_z):
         core_copy(p).wait_send()
-        half_copy(p, p % 2 == 0, 0).wait_send()
-        half_copy(p, p % 2 == 0, 1).wait_send()
-        quarter_copy(p, p % 2 == 0).wait_send()
+        half_copy(p, p >= n_z // 2, 0).wait_send()
+        half_copy(p, p >= n_z // 2, 1).wait_send()
+        quarter_copy(p, p >= n_z // 2).wait_send()
 
         @pl.when(p != z)
         def _(p=p):
-            chain_copy(p, 0).wait_send()
+            chain_copy(p).wait_send()
 
     for i in range(3):
         ag_copy(i, f).wait_send()
@@ -385,20 +396,22 @@
             pltpu.VMEM((n_z, n_tok, width), BF16),
             pltpu.VMEM((n_z, 2, qr, width), BF16),
             pltpu.VMEM((n_z, qr, width), BF16),
-            pltpu.VMEM((n_z, 2, qr, width), BF16),
+            pltpu.VMEM((n_z, qr, width), BF16),
             pltpu.VMEM((3, hid, width), BF16),
             pltpu.VMEM((hid, width), F32),
             pltpu.VMEM((hid, width), BF16),
             pltpu.VMEM((hid_all, cols), BF16),
-            dma((5,)), dma((2, n_z, 4)), dma((2, n_z, 2)), dma((2, n_z, 2)), dma((2, n_z)),
+            pltpu.VMEM((hid_all, cols), BF16),
+            pltpu.VMEM((hid_all, cols), BF16),
+            dma((2,)), dma((2, n_z, 4)), dma((2, n_z, 2)), dma((2, n_z, 2)), dma((2, n_z)),
             dma((2, n_z)), dma((2, n_z)), dma((3, n_tp)), dma((3, n_tp)), dma((n_z,)), dma((n_z,)),
-            dma((n_z, 2)), dma((n_z, 2)), dma((n_z,)), dma((n_z,)), dma((n_z,)), dma((n_z, 2)),
+            dma((n_z, 2)), dma((n_z, 2)), dma((n_z,)), dma((n_z,)), dma((n_z,)), dma((n_z,)),
             dma((3,)), dma((3,)), dma((n_tp,)), dma((n_tp,)),
         ],
         compiler_params=pltpu.CompilerParams(
             collective_id=0, has_side_effects=True, vmem_limit_bytes=66_000_000
         ),
-    )(inputs, cotangent, gate_weight.T, up_weight.T, down_weight)
+    )(inputs, cotangent, gate_weight, up_weight, down_weight)
 
 
 def solution(mesh):

time: 222 us -> 194 us (0.87)
  Pallas kernels: 212 us -> 190 us
  local copies, waits for them, and re-layouts: 7.19 us -> 3.73 us
    pallas_call x1, Pallas kernels: 212 us -> 190 us  [spread(): pl.pallas_call(functools.partial(kernel, n_tp), name='spread_hidden', out...]
    unnamed x8 -> x4, local copies, waits for them, and re-layouts: 7.19 us -> 3.73 us
where the time goes in v2:
time: 194 us
  Pallas kernels  190 us (98%)
  local copies, waits for them, and re-layouts  3.73 us (2%)
    pallas_call x1, Pallas kernels, spread(): pl.pallas_call(functools.partial(kernel, n_tp), name='spread_hidden', out...  190 us

profile of v2, /device:TPU:8, one launch (start us, length us, event | category | flops | bytes accessed | tf_op | source)
XLA Modules:
  0.0 194.2 jit_solution(14663290262640074411)
XLA Ops:
  0.6 189.8 %spread_hidden.1 = (bf16[1,320,2048]{2,1,0:T(8,128)(2,1)}, f32[1408,256]{1,0:T(8,128)}) custom-call(bf16[1,320,2048]{2,1,0:T(8,128)(2,1)} %x_ref.1, bf16[1,320,2048]{2,1,0:T(8,128)(2,1)} %ct_ref.1, bf16[256,1408]{1,0:T(8,128)(2,1)} %wg_ref.1, bf16[256,1408]{1,0:T(8,128)(2,1)} %wu_ref.1, bf16[1408,256]{1,0:T(8,128)(2,1)} %wd_ref.1), custom_call_target="tpu_custom_call" | custom-call | tf_op jit(solution)/shard_map/spread_hidden/pallas_call | solution.py:384
  190.4 0.0 copy-start
  190.5 2.6 %copy.9 = bf16[1,320,2048]{2,1,0:T(8,128)(2,1)} copy(bf16[1,320,2048]{2,1,0:T(8,128)(2,1)} %get-tuple-element.4) | data formatting | bytes 2621440
  193.1 0.0 copy-done
  193.1 1.1 copy.10
Async XLA Ops:
  190.4 2.6 %copy-start = (f32[1408,256]{1,0:T(8,128)S(1)}, f32[1408,256]{1,0:T(8,128)}, u32[]{:S(2)}) copy-start(f32[1408,256]{1,0:T(8,128)} %get-tuple-element.5) | copy-start | bytes 4325380

commit v3 on v2

--- a/solution.py
+++ b/solution.py
@@ -211,10 +211,16 @@
     def core_copy(p):
         return rc(part.at[p * 2 + 1 - c], core_in.at[p], core_ss.at[p], core_rs.at[p], partner)
 
+    def side(first_x):
+        return pl.ds(width // 2 if first_x else 0, width // 2)
+
     def half_copy(p, first_x, i):
-        q = jnp.where(first_x, i * 2 + (1 - fx), (1 - fy) * 2 + i)
-        dev = {"fs": jnp.where(first_x, f_x, f_y)}
-        return rc(part.at[p * 2 + c, qs(q)], half_in.at[p, i], half_ss.at[p, i], half_rs.at[p, i], dev)
+        q = i * 2 + (1 - fx) if first_x else (1 - fy) * 2 + i
+        return rc(
+            part.at[p * 2 + c, qs(q), side(first_x)], half_in.at[p, i, :, side(first_x)],
+            half_ss.at[p, i, int(first_x)], half_rs.at[p, i, int(first_x)],
+            dev_x if first_x else dev_y,
+        )
 
     @pl.loop(0, n_z)
     def _(j):
@@ -248,9 +254,9 @@
         core_copy(p).wait_recv()
         s = p * 2 + c
         part[s] = (part[s].astype(F32) + core_in[p].astype(F32)).astype(BF16)
-        first_x = p >= n_z // 2
-        half_copy(p, first_x, 0).start()
-        half_copy(p, first_x, 1).start()
+        for i in range(2):
+            half_copy(p, True, i).start()
+            half_copy(p, False, i).start()
 
     down_out[...] = acc[...].astype(BF16)
 
@@ -266,25 +272,27 @@
         dn_copy(k).start()
 
     def quarter_copy(p, first_x):
-        q = jnp.where(first_x, f_y, f_x)
-        return rc(
-            part.at[p * 2 + c, qs(q)], quarter_in.at[p], q_ss.at[p], q_rs.at[p],
-            {"fs": jnp.where(first_x, f_y, f_x)},
+        return rc(
+            part.at[p * 2 + c, qs(f_y if first_x else f_x), side(first_x)],
+            quarter_in.at[p, :, side(first_x)],
+            q_ss.at[p, int(first_x)], q_rs.at[p, int(first_x)], dev_y if first_x else dev_x,
         )
 
     def half_add(p):
-        first_x = p >= n_z // 2
         s = p * 2 + c
-        other = jnp.where(first_x, 1 - fy, 1 - fx)
-        mine = jnp.where(first_x, fy, fx)
-        for i in range(2):
-            half_copy(p, first_x, i).wait_recv()
-        q_other = jnp.where(first_x, f_y, f_x)
-        part[s, qs(q_other)] = (
-            part[s, qs(q_other)].astype(F32) + half_in[p, other].astype(F32)
-        ).astype(BF16)
-        quarter_copy(p, first_x).start()
-        part[s, qs(f)] = (part[s, qs(f)].astype(F32) + half_in[p, mine].astype(F32)).astype(BF16)
+        for first_x in (True, False):
+            mine = fy if first_x else fx
+            half = side(first_x)
+            for i in range(2):
+                half_copy(p, first_x, i).wait_recv()
+            q_other = f_y if first_x else f_x
+            part[s, qs(q_other), half] = (
+                part[s, qs(q_other), half].astype(F32) + half_in[p, 1 - mine, :, half].astype(F32)
+            ).astype(BF16)
+            quarter_copy(p, first_x).start()
+            part[s, qs(f), half] = (
+                part[s, qs(f), half].astype(F32) + half_in[p, mine, :, half].astype(F32)
+            ).astype(BF16)
 
     def chain_copy(p):
         return rc(
@@ -300,7 +308,8 @@
         @pl.when(j > 0)
         def _():
             p = sweep(j - 1)
-            quarter_copy(p, p >= n_z // 2).wait_recv()
+            quarter_copy(p, True).wait_recv()
+            quarter_copy(p, False).wait_recv()
             s = p * 2 + c
             part[s, qs(f)] = (part[s, qs(f)].astype(F32) + quarter_in[p].astype(F32)).astype(BF16)
 
@@ -362,9 +371,10 @@
         dn_copy(k).wait_send()
     for p in range(n_z):
         core_copy(p).wait_send()
-        half_copy(p, p >= n_z // 2, 0).wait_send()
-        half_copy(p, p >= n_z // 2, 1).wait_send()
-        quarter_copy(p, p >= n_z // 2).wait_send()
+        for first_x in (True, False):
+            half_copy(p, first_x, 0).wait_send()
+            half_copy(p, first_x, 1).wait_send()
+            quarter_copy(p, first_x).wait_send()
 
         @pl.when(p != z)
         def _(p=p):
@@ -405,7 +415,7 @@
             pltpu.VMEM((hid_all, cols), BF16),
             dma((2,)), dma((2, n_z, 4)), dma((2, n_z, 2)), dma((2, n_z, 2)), dma((2, n_z)),
             dma((2, n_z)), dma((2, n_z)), dma((3, n_tp)), dma((3, n_tp)), dma((n_z,)), dma((n_z,)),
-            dma((n_z, 2)), dma((n_z, 2)), dma((n_z,)), dma((n_z,)), dma((n_z,)), dma((n_z,)),
+            dma((n_z, 2, 2)), dma((n_z, 2, 2)), dma((n_z, 2)), dma((n_z, 2)), dma((n_z,)), dma((n_z,)),
             dma((3,)), dma((3,)), dma((n_tp,)), dma((n_tp,)),
         ],
         compiler_params=pltpu.CompilerParams(

time: 194 us -> 187 us (0.964)
  Pallas kernels: 190 us -> 182 us
    pallas_call x1, Pallas kernels: 190 us -> 182 us  [spread(): pl.pallas_call(functools.partial(kernel, n_tp), name='spread_hidden', out...]
where the time goes in v3:
time: 187 us; the launch traced here: 186 us
  Pallas kernels  182 us (97%)
  local copies, waits for them, and re-layouts  3.73 us (2%)
    pallas_call x1, Pallas kernels, spread(): pl.pallas_call(functools.partial(kernel, n_tp), name='spread_hidden', out...  182 us

profile of v3, /device:TPU:8, one launch (start us, length us, event | category | flops | bytes accessed | tf_op | source)
XLA Modules:
  0.0 186.0 jit_solution(9930806432001983336)
XLA Ops:
  0.6 181.6 %spread_hidden.1 = (bf16[1,320,2048]{2,1,0:T(8,128)(2,1)}, f32[1408,256]{1,0:T(8,128)}) custom-call(bf16[1,320,2048]{2,1,0:T(8,128)(2,1)} %x_ref.1, bf16[1,320,2048]{2,1,0:T(8,128)(2,1)} %ct_ref.1, bf16[256,1408]{1,0:T(8,128)(2,1)} %wg_ref.1, bf16[256,1408]{1,0:T(8,128)(2,1)} %wu_ref.1, bf16[1408,256]{1,0:T(8,128)(2,1)} %wd_ref.1), custom_call_target="tpu_custom_call" | custom-call | tf_op jit(solution)/shard_map/spread_hidden/pallas_call | solution.py:394
  182.3 0.0 copy-start
  182.3 2.6 %copy.9 = bf16[1,320,2048]{2,1,0:T(8,128)(2,1)} copy(bf16[1,320,2048]{2,1,0:T(8,128)(2,1)} %get-tuple-element.4) | data formatting | bytes 2621440
  184.9 0.0 copy-done
  184.9 1.1 copy.10
Async XLA Ops:
  182.3 2.6 %copy-start = (f32[1408,256]{1,0:T(8,128)S(1)}, f32[1408,256]{1,0:T(8,128)}, u32[]{:S(2)}) copy-start(f32[1408,256]{1,0:T(8,128)} %get-tuple-element.5) | copy-start | bytes 4325380
